TPU v7x, 32 devices: a whole 2x2x4 slice. The times are simulated.
32 devices in a mesh: grp: 2 (over y), ep: 8 (over z, core), tp: 2 (over x).
Axes of the slice: x: 2, y: 2, z: 4, core: 2. Of those that a mesh axis runs over, the one named last changes fastest.
Arguments:
- tokens: bfloat16 [512, 2048], P(('grp', 'ep')), parts along dimension 0, may hold values from -12 to 12
- routes: int32 [512, 4], P(('grp', 'ep')), parts along dimension 0, may hold values from 0 to 7, all different within a row; in each aligned block of 32 rows (0 to 31, 32 to 63, ...) at most 32 rows name the same one
- gates: float32 [512, 4], P(('grp', 'ep')), parts along dimension 0, may hold values from 0.1 to 1
- norm_gain: bfloat16 [2048], replicated, may hold values from 0.099609375 to 1.8984375
- exp_gate: bfloat16 [8, 2048, 2048], P('ep', None, 'tp'), may hold values from -0.125 to 0.125
- exp_up: bfloat16 [8, 2048, 2048], P('ep', None, 'tp'), may hold values from -0.125 to 0.125
- exp_down: bfloat16 [8, 2048, 2048], P('ep', 'tp'), may hold values from -0.26516504 to 0.26516504
- sh_gate: bfloat16 [2048, 1024], P(None, 'tp'), may hold values from -0.125 to 0.125
- sh_up: bfloat16 [2048, 1024], P(None, 'tp'), may hold values from -0.125 to 0.125
- sh_down: bfloat16 [1024, 2048], P('tp'), may hold values from -0.375 to 0.375
- out_gain: bfloat16 [2048], P('tp'), may hold values from 0.099609375 to 1.8984375
Outputs:
- mixed: bfloat16 [512, 2048], P(('grp', 'ep'), 'tp'), parts along dimension 0
There are 2 independent parts, one for each index of `grp`. A program takes and returns all parts, laid end to end along the dimension named above; an argument that names none is the same for every part. Nothing has to cross between parts.
Inputs may be any that keep to these rules, and one draw needn't show every extreme that they name: `routes`: each row names 4 different experts; within the rows of one device (aligned blocks of 32 rows) no expert is named by more than 32 rows, a bound that some block reaches.
All inputs are finite; a program needn't handle non-finite values.
Results may differ from a plain program's by a relative error of at most 0.015.
Values may be sent and summed in bfloat16 or wider, within the bound.
A program may use at most 64 MiB of HBM per device.

v0:
```python
import functools

import jax
import jax.numpy as jnp
from jax import lax
from jax.experimental import pallas as pl
from jax.experimental.pallas import tpu as pltpu
from jax.sharding import PartitionSpec as P

EPSILON = 1e-06
MESH = pl.DeviceIdType.MESH
F32 = jnp.float32
BF16 = jnp.bfloat16


def silu(v):
    return v / (1.0 + jnp.exp(-v))


def kernel(
    n_ep, n_tp, experts,
    tok_ref, routes_ref, gates_ref, ngain_ref, wg_hbm, wu_hbm, wd_hbm, sg_hbm, su_hbm, sd_hbm, ogain_ref,
    out_ref,
    wg, wu, wd, sg, su, sd, xs, hid, shid, shp, d_out, d_in, x_out, x_in, acc, z_out, z_in, q_out, q_in,
    w_sem, disp_send, disp_recv, fwd_send, fwd_recv, d_send, d_recv, x_send, x_recv, z_send, z_recv, q_send, q_recv,
):
    nz = n_ep // 2
    me = lax.axis_index("ep")
    t = lax.axis_index("tp")
    z, c = me // 2, lax.rem(me, 2)
    other = 1 - c
    T, D = tok_ref.shape
    F = wg.shape[1]
    S = sg.shape[1]
    Dt = D // n_tp
    rows = nz * T
    pad = xs.shape[3] - D

    loads = []
    for i, (src, dst) in enumerate(
        ((sg_hbm, sg), (su_hbm, su), (sd_hbm, sd), (wg_hbm.at[0], wg), (wu_hbm.at[0], wu), (wd_hbm.at[0], wd))
    ):
        copy = pltpu.make_async_copy(src, dst, w_sem.at[i])
        copy.start()
        loads.append(copy)

    def zpeer(dz):
        peer = z
        for bit in range(dz.bit_length()):
            if dz >> bit & 1:
                peer = peer + (1 << bit) * (1 - 2 * lax.rem(z // (1 << bit), 2))
        return peer

    def tpeer(j):
        return lax.rem(t + j, n_tp)

    partner = {"ep": z * 2 + other}
    barrier = pltpu.get_barrier_semaphore()
    peers = [{"ep": zpeer(dz) * 2 + c} for dz in range(1, nz)] + [partner]
    peers += [{"tp": tpeer(j)} for j in range(1, n_tp)]
    for peer in peers:
        pl.semaphore_signal(barrier, inc=1, device_id=peer, device_id_type=MESH)

    def remote(src, dst, ssem, rsem, device):
        return pltpu.make_async_remote_copy(
            src_ref=src, dst_ref=dst, send_sem=ssem, recv_sem=rsem, device_id=device, device_id_type=MESH
        )

    values = tok_ref[...].astype(F32)
    scale = lax.rsqrt(jnp.mean(values * values, axis=1, keepdims=True) + EPSILON)
    normed = (values * scale * ngain_ref[...].astype(F32).reshape(1, D)).astype(BF16)
    row = lax.broadcasted_iota(jnp.int32, (pad, T), 0)
    row_expert = lax.rem(row, experts)
    dense = jnp.zeros((pad, T), F32)
    for k in range(routes_ref.shape[0]):
        dense = dense + jnp.where(row_expert == routes_ref[k : k + 1, :], gates_ref[k : k + 1, :], 0.0)
    high = dense.astype(BF16).astype(F32)
    rest = dense - high
    mid = rest.astype(BF16).astype(F32)
    part = row // experts
    packed = jnp.where(part == 0, high, jnp.where(part == 1, mid, jnp.where(part == 2, rest - mid, 0.0)))
    packed = packed.T
    xs[c, z, :, :D] = normed
    xs[c, z, :, D:] = packed.astype(BF16)

    pl.semaphore_wait(barrier, len(peers))

    own = xs.at[c, z]
    sends = []
    order = list(range(nz - 1, 0, -1))
    for dz in order:
        copy = remote(own, own, disp_send.at[dz], disp_recv.at[dz], {"ep": zpeer(dz) * 2 + c})
        copy.start()
        sends.append(copy)
    first = remote(own, own, fwd_send.at[0], fwd_recv.at[0], partner)
    first.start()

    loads[0].wait()
    loads[1].wait()
    tile = min(256, S)

    @pl.loop(0, S // tile)
    def _(i):
        cols = pl.ds(pl.multiple_of(i * tile, tile), tile)
        x = xs[c, z, :, :D]
        g = jnp.dot(x, sg[:, cols], preferred_element_type=F32)
        u = jnp.dot(x, su[:, cols], preferred_element_type=F32)
        shid[:, cols] = (silu(g) * u).astype(BF16)

    loads[2].wait()
    dtile = min(512, Dt)

    @pl.loop(0, D // dtile)
    def _(i):
        cols = pl.ds(pl.multiple_of(i * dtile, dtile), dtile)
        shp[:, cols] = jnp.dot(shid[...], sd[:, cols], preferred_element_type=F32)

    forwards = [first]
    for dz in range(1, nz):
        src_z = zpeer(dz)
        block = xs.at[c, src_z]
        remote(block, block, disp_send.at[dz], disp_recv.at[dz], partner).wait_recv()
        copy = remote(block, block, fwd_send.at[dz], fwd_recv.at[dz], partner)
        copy.start()
        forwards.append(copy)

    loads[3].wait()
    loads[4].wait()
    ftile = min(512, F)
    glane = lax.broadcasted_iota(jnp.int32, (rows, pad), 1)
    mine = (lax.rem(glane, experts) == me) & (glane < 3 * experts)

    def hidden(half, slot):
        packed_gates = xs[half, :, :, D:].reshape(rows, pad).astype(F32)
        weight = jnp.sum(jnp.where(mine, packed_gates, 0.0), axis=1, keepdims=True)

        @pl.loop(0, F // ftile)
        def _(i):
            cols = pl.ds(pl.multiple_of(i * ftile, ftile), ftile)
            x = xs[half, :, :, :D].reshape(rows, D)
            g = jnp.dot(x, wg[:, cols], preferred_element_type=F32)
            u = jnp.dot(x, wu[:, cols], preferred_element_type=F32)
            hid[slot, :, cols] = (silu(g) * u * weight).astype(BF16)

    hidden(c, 0)
    for dz in range(nz):
        src_z = zpeer(dz)
        block = xs.at[other, src_z]
        remote(block, block, fwd_send.at[dz], fwd_recv.at[dz], partner).wait_recv()
    hidden(other, 1)
    loads[5].wait()

    def down(slot, tp, store):
        @pl.loop(0, Dt // dtile)
        def _(i):
            src = pl.ds(pl.multiple_of(tp * Dt + i * dtile, dtile), dtile)
            dst = pl.ds(pl.multiple_of(i * dtile, dtile), dtile)
            store(src, dst, jnp.dot(hid[slot], wd[:, src], preferred_element_type=F32))

    js = list(range(1, n_tp)) + [0]
    d_copies = {}
    x_copies = {}
    for j in js:
        def store(src, dst, value):
            d_out[j, :, :, dst] = value.astype(BF16).reshape(nz, T, dtile)

        down(1, tpeer(j), store)
        copy = remote(d_out.at[j], d_in.at[j], d_send.at[j], d_recv.at[j], partner)
        copy.start()
        d_copies[j] = copy

        def keep(src, dst, value):
            acc[:, :, dst] = value.reshape(nz, T, dtile)
            acc[z, :, dst] += shp[:, src]

        down(0, tpeer(j), keep)
        d_copies[j].wait_recv()
        if j == 0:
            acc[...] += d_in[j].astype(F32)
        else:
            for dz in order + [0]:
                zt = zpeer(dz)
                x_out[j, zt] = (acc[zt] + d_in[j, zt].astype(F32)).astype(BF16)
                copy = remote(
                    x_out.at[j, zt], x_in.at[j, zt], x_send.at[j, dz], x_recv.at[j, dz], {"tp": tpeer(j)}
                )
                copy.start()
                x_copies[j, dz] = copy

    z_copies = {}
    for dz in order + [0]:
        zt = zpeer(dz)
        total = acc[zt]
        for j in range(1, n_tp):
            x_copies[j, dz].wait_recv()
            total = total + x_in[j, zt].astype(F32)
        if dz == 0:
            acc[zt] = total
        else:
            z_out[dz] = total.astype(BF16)
            copy = remote(z_out.at[dz], z_in.at[dz], z_send.at[dz], z_recv.at[dz], {"ep": zt * 2 + c})
            copy.start()
            z_copies[dz] = copy

    total = acc[z]
    for dz in range(1, nz):
        z_copies[dz].wait_recv()
        total = total + z_in[dz].astype(F32)
    squares = jnp.sum(total * total, axis=1, keepdims=True)
    q_out[...] = jnp.broadcast_to(squares, q_out.shape)
    q_copies = []
    for j in range(1, n_tp):
        copy = remote(q_out, q_in.at[j], q_send.at[j], q_recv.at[j], {"tp": tpeer(j)})
        copy.start()
        q_copies.append(copy)
    gained = total * ogain_ref[...].astype(F32).reshape(1, Dt)
    for j, copy in enumerate(q_copies):
        copy.wait_recv()
        squares = squares + q_in[j + 1, :, :1]
    out_ref[...] = (gained * lax.rsqrt(squares / D + EPSILON)).astype(BF16)

    for copy in sends + forwards + list(d_copies.values()) + list(x_copies.values()) + list(z_copies.values()) + q_copies:
        copy.wait_send()


def solution(mesh):
    n_ep, n_tp = mesh.shape["ep"], mesh.shape["tp"]
    nz = n_ep // 2

    def shards(tokens, routes, gates, norm_gain, exp_gate, exp_up, exp_down, sh_gate, sh_up, sh_down, out_gain):
        T, D = tokens.shape
        local, _, F = exp_gate.shape
        S = sh_gate.shape[1]
        assert local == 1
        experts = local * n_ep
        Dt = D // n_tp
        pad = 128 * ((3 * experts + 127) // 128)
        vmem = pl.BlockSpec(memory_space=pltpu.VMEM)
        hbm = pl.BlockSpec(memory_space=pl.ANY)
        dma = pltpu.SemaphoreType.DMA
        return pl.pallas_call(
            functools.partial(kernel, n_ep, n_tp, experts),
            out_shape=jax.ShapeDtypeStruct((T, Dt), BF16),
            in_specs=[vmem] * 4 + [hbm] * 6 + [vmem],
            out_specs=vmem,
            scratch_shapes=[
                pltpu.VMEM((D, F), BF16),
                pltpu.VMEM((D, F), BF16),
                pltpu.VMEM((F, D), BF16),
                pltpu.VMEM((D, S), BF16),
                pltpu.VMEM((D, S), BF16),
                pltpu.VMEM((S, D), BF16),
                pltpu.VMEM((2, nz, T, D + pad), BF16),
                pltpu.VMEM((2, nz * T, F), BF16),
                pltpu.VMEM((T, S), BF16),
                pltpu.VMEM((T, D), F32),
                pltpu.VMEM((n_tp, nz, T, Dt), BF16),
                pltpu.VMEM((n_tp, nz, T, Dt), BF16),
                pltpu.VMEM((n_tp, nz, T, Dt), BF16),
                pltpu.VMEM((n_tp, nz, T, Dt), BF16),
                pltpu.VMEM((nz, T, Dt), F32),
                pltpu.VMEM((nz, T, Dt), BF16),
                pltpu.VMEM((nz, T, Dt), BF16),
                pltpu.VMEM((T, 128), F32),
                pltpu.VMEM((n_tp, T, 128), F32),
                dma((6,)),
                dma((nz,)), dma((nz,)), dma((nz,)), dma((nz,)),
                dma((n_tp,)), dma((n_tp,)),
                dma((n_tp, nz)), dma((n_tp, nz)),
                dma((nz,)), dma((nz,)),
                dma((n_tp,)), dma((n_tp,)),
            ],
            compiler_params=pltpu.CompilerParams(collective_id=0, has_side_effects=True),
        )(
            tokens, routes.T, gates.T, norm_gain, exp_gate, exp_up, exp_down,
            sh_gate, sh_up, sh_down, out_gain,
        )

    placed = (
        P(("grp", "ep"), None),
        P(("grp", "ep"), None),
        P(("grp", "ep"), None),
        P(),
        P("ep", None, "tp"),
        P("ep", None, "tp"),
        P("ep", "tp", None),
        P(None, "tp"),
        P(None, "tp"),
        P("tp", None),
        P("tp"),
    )
    return jax.shard_map(
        shards, mesh=mesh, in_specs=placed, out_specs=P(("grp", "ep"), "tp"), check_vma=False
    )
```

profile of v0, /device:TPU:0, one launch (start us, length us, event | category | flops | bytes accessed | tf_op | source)
XLA Modules:
  0.0 39.2 jit_solution(3172883438966516069)
XLA Ops:
  0.0 37.7 %shard_map.109 = bf16[32,1024]{1,0:T(8,128)(2,1)} custom-call(bf16[32,2048]{1,0:T(8,128)(2,1)} %tok_ref.1, s32[4,32]{1,0:T(4,128)} %bitcast.2, f32[4,32]{1,0:T(4,128)} %bitcast.3, bf16[2048]{0:T(1024)(128)(2,1)} %ngain_ref.1, bf16[1,2048,1024]{2,1,0:T(8,128)(2,1)} %wg_hbm.1, bf16[1,2048,1024]{2,1,0:T(8,128)(2,1)} %wu_hbm.1, bf16[1,1024,2048]{2,1,0:T(8,128)(2,1)} %wd_hbm.1, ...), custom_call_target="tpu_custom_call" | custom-call | tf_op jit(solution)/shard_map/pallas_call | solution.py:241
  37.7 1.5 %copy.13 = bf16[32,1024]{1,0:T(8,128)(2,1)} copy(bf16[32,1024]{1,0:T(8,128)(2,1)} %shard_map.109) | data formatting | bytes 131072
where the time goes:
time: 39.3 us; the launch traced here: 39.2 us
  Pallas kernels  37.7 us (96%)
  local copies, waits for them, and re-layouts  1.47 us (4%)
    pallas_call x1, Pallas kernels, shards(): pl.pallas_call(functools.partial(kernel, n_ep, n_tp, experts), out_shape=...  37.7 us
    unnamed x1, local copies, waits for them, and re-layouts  1.47 us

commit v1 on v0

v1 whole, which is shorter than its diff:
```python
import functools

import jax
import jax.numpy as jnp
from jax import lax
from jax.experimental import pallas as pl
from jax.experimental.pallas import tpu as pltpu
from jax.sharding import PartitionSpec as P

EPSILON = 1e-06
MESH = pl.DeviceIdType.MESH
F32 = jnp.float32
BF16 = jnp.bfloat16


def silu(v):
    return v / (1.0 + jnp.exp(-v))


def kernel(
    n_ep, n_tp, experts,
    tok_ref, routes_ref, gates_ref, ngain_ref, wg_hbm, wu_hbm, wd_hbm, sg_hbm, su_hbm, sd_hbm, ogain_ref,
    out_ref,
    wg, wu, wd, sg, su, sd, xs, hid, shid, shp, d_out, d_in, x_out, x_in, acc, z_out, z_in, q_out, q_in,
    w_sem, disp_send, disp_recv, fwd_send, fwd_recv, d_send, d_recv, x_send, x_recv, z_send, z_recv, q_send, q_recv,
):
    nz = n_ep // 2
    me = lax.axis_index("ep")
    t = lax.axis_index("tp")
    z, c = me // 2, lax.rem(me, 2)
    other = 1 - c
    T, D = tok_ref.shape
    F = wg.shape[1]
    S = sg.shape[1]
    Dt = D // n_tp
    rows = 2 * T
    pad = xs.shape[3] - D

    loads = []
    for i, (src, dst) in enumerate(
        ((sg_hbm, sg), (su_hbm, su), (sd_hbm, sd), (wg_hbm.at[0], wg), (wu_hbm.at[0], wu), (wd_hbm.at[0], wd))
    ):
        copy = pltpu.make_async_copy(src, dst, w_sem.at[i])
        copy.start()
        loads.append(copy)

    def zpeer(dz):
        peer = z
        for bit in range(dz.bit_length()):
            if dz >> bit & 1:
                peer = peer + (1 << bit) * (1 - 2 * lax.rem(z // (1 << bit), 2))
        return peer

    def tpeer(j):
        return lax.rem(t + j, n_tp)

    partner = {"ep": z * 2 + other}
    barrier = pltpu.get_barrier_semaphore()
    peers = [{"ep": zpeer(dz) * 2 + c} for dz in range(1, nz)] + [partner]
    peers += [{"tp": tpeer(j)} for j in range(1, n_tp)]
    for peer in peers:
        pl.semaphore_signal(barrier, inc=1, device_id=peer, device_id_type=MESH)

    def remote(src, dst, ssem, rsem, device):
        return pltpu.make_async_remote_copy(
            src_ref=src, dst_ref=dst, send_sem=ssem, recv_sem=rsem, device_id=device, device_id_type=MESH
        )

    values = tok_ref[...].astype(F32)
    scale = lax.rsqrt(jnp.mean(values * values, axis=1, keepdims=True) + EPSILON)
    normed = (values * scale * ngain_ref[...].astype(F32).reshape(1, D)).astype(BF16)
    row = lax.broadcasted_iota(jnp.int32, (pad, T), 0)
    row_expert = lax.rem(row, experts)
    dense = jnp.zeros((pad, T), F32)
    for k in range(routes_ref.shape[0]):
        dense = dense + jnp.where(row_expert == routes_ref[k : k + 1, :], gates_ref[k : k + 1, :], 0.0)
    high = dense.astype(BF16).astype(F32)
    rest = dense - high
    mid = rest.astype(BF16).astype(F32)
    part = row // experts
    packed = jnp.where(part == 0, high, jnp.where(part == 1, mid, jnp.where(part == 2, rest - mid, 0.0)))
    packed = packed.T
    xs[z, c, :, :D] = normed
    xs[z, c, :, D:] = packed.astype(BF16)

    pl.semaphore_wait(barrier, len(peers))

    sent = []

    def send(src, dst, ssem, rsem, device):
        copy = remote(src, dst, ssem, rsem, device)
        copy.start()
        sent.append(copy)
        return copy

    order = list(range(nz - 1, 0, -1))
    js = list(range(1, n_tp)) + [0]
    own = xs.at[z, c]
    for dz in order:
        send(own, own, disp_send.at[dz], disp_recv.at[dz], {"ep": zpeer(dz) * 2 + c})
    send(own, own, fwd_send.at[0], fwd_recv.at[0], partner)

    dtile = min(512, Dt)

    def shared():
        loads[0].wait()
        loads[1].wait()
        tile = min(256, S)

        @pl.loop(0, S // tile)
        def _(i):
            cols = pl.ds(pl.multiple_of(i * tile, tile), tile)
            x = xs[z, c, :, :D]
            g = jnp.dot(x, sg[:, cols], preferred_element_type=F32)
            u = jnp.dot(x, su[:, cols], preferred_element_type=F32)
            shid[:, cols] = (silu(g) * u).astype(BF16)

        loads[2].wait()

        @pl.loop(0, D // dtile)
        def _(i):
            cols = pl.ds(pl.multiple_of(i * dtile, dtile), dtile)
            shp[:, cols] = jnp.dot(shid[...], sd[:, cols], preferred_element_type=F32)

    def arrive(dz):
        block = xs.at[zpeer(dz), c]
        remote(block, block, disp_send.at[dz], disp_recv.at[dz], partner).wait_recv()
        send(block, block, fwd_send.at[dz], fwd_recv.at[dz], partner)

    ftile = min(512, F)
    glane = lax.broadcasted_iota(jnp.int32, (rows, pad), 1)
    mine = (lax.rem(glane, experts) == me) & (glane < 3 * experts)

    def hidden(dz):
        src_z = zpeer(dz)
        block = xs.at[src_z, other]
        remote(block, block, fwd_send.at[dz], fwd_recv.at[dz], partner).wait_recv()
        packed_gates = xs[src_z, :, :, D:].reshape(rows, pad).astype(F32)
        weight = jnp.sum(jnp.where(mine, packed_gates, 0.0), axis=1, keepdims=True)

        @pl.loop(0, F // ftile)
        def _(i):
            cols = pl.ds(pl.multiple_of(i * ftile, ftile), ftile)
            x = xs[src_z, :, :, :D].reshape(rows, D)
            g = jnp.dot(x, wg[:, cols], preferred_element_type=F32)
            u = jnp.dot(x, wu[:, cols], preferred_element_type=F32)
            hid[:, :, cols] = (silu(g) * u * weight).astype(BF16).reshape(2, T, ftile)

    def down(dz):
        src_z = zpeer(dz)
        for j in js:
            @pl.loop(0, Dt // dtile)
            def _(i):
                src = pl.ds(pl.multiple_of(tpeer(j) * Dt + i * dtile, dtile), dtile)
                dst = pl.ds(pl.multiple_of(i * dtile, dtile), dtile)
                h = hid[...].reshape(rows, F)
                both = jnp.dot(h, wd[:, src], preferred_element_type=F32).reshape(2, T, dtile)
                mine_first = c == 0
                keep = jnp.where(mine_first, both[0], both[1])
                give = jnp.where(mine_first, both[1], both[0])
                d_out[j, src_z, :, dst] = give.astype(BF16)
                if dz == 0:
                    keep = keep + shp[:, src]
                acc[j, src_z, :, dst] = keep

            send(d_out.at[j, src_z], d_in.at[j, src_z], d_send.at[j, dz], d_recv.at[j, dz], partner)

    def pair(dz):
        src_z = zpeer(dz)
        for j in js:
            remote(d_out.at[j, src_z], d_in.at[j, src_z], d_send.at[j, dz], d_recv.at[j, dz], partner).wait_recv()
            total = acc[j, src_z] + d_in[j, src_z].astype(F32)
            if j == 0:
                acc[0, src_z] = total
            else:
                x_out[j, src_z] = total.astype(BF16)
                send(x_out.at[j, src_z], x_in.at[j, src_z], x_send.at[j, dz], x_recv.at[j, dz], {"tp": tpeer(j)})

    def finish(dz):
        src_z = zpeer(dz)
        total = acc[0, src_z]
        for j in range(1, n_tp):
            remote(
                x_out.at[j, src_z], x_in.at[j, src_z], x_send.at[j, dz], x_recv.at[j, dz], {"tp": tpeer(j)}
            ).wait_recv()
            total = total + x_in[j, src_z].astype(F32)
        if dz == 0:
            acc[0, src_z] = total
        else:
            z_out[dz] = total.astype(BF16)
            send(z_out.at[dz], z_in.at[dz], z_send.at[dz], z_recv.at[dz], {"ep": src_z * 2 + c})

    shared()
    for load in loads[3:]:
        load.wait()
    hidden(0)
    down(0)
    slots = [0] + order
    for i, dz in enumerate(order):
        arrive(dz)
        pair(slots[i])
        hidden(dz)
        down(dz)
        if i:
            finish(slots[i - 1])
    pair(slots[-1])
    for dz in slots[-2:]:
        finish(dz)

    total = acc[0, z]
    for dz in order:
        remote(z_out.at[dz], z_in.at[dz], z_send.at[dz], z_recv.at[dz], partner).wait_recv()
        total = total + z_in[dz].astype(F32)
    squares = jnp.sum(total * total, axis=1, keepdims=True)
    q_out[...] = jnp.broadcast_to(squares, q_out.shape)
    q_copies = []
    for j in range(1, n_tp):
        q_copies.append(send(q_out, q_in.at[j], q_send.at[j], q_recv.at[j], {"tp": tpeer(j)}))
    gained = total * ogain_ref[...].astype(F32).reshape(1, Dt)
    for j, copy in enumerate(q_copies):
        copy.wait_recv()
        squares = squares + q_in[j + 1, :, :1]
    out_ref[...] = (gained * lax.rsqrt(squares / D + EPSILON)).astype(BF16)

    for copy in sent:
        copy.wait_send()


def solution(mesh):
    n_ep, n_tp = mesh.shape["ep"], mesh.shape["tp"]
    nz = n_ep // 2

    def shards(tokens, routes, gates, norm_gain, exp_gate, exp_up, exp_down, sh_gate, sh_up, sh_down, out_gain):
        T, D = tokens.shape
        local, _, F = exp_gate.shape
        S = sh_gate.shape[1]
        assert local == 1
        experts = local * n_ep
        Dt = D // n_tp
        pad = 128 * ((3 * experts + 127) // 128)
        vmem = pl.BlockSpec(memory_space=pltpu.VMEM)
        hbm = pl.BlockSpec(memory_space=pl.ANY)
        dma = pltpu.SemaphoreType.DMA
        return pl.pallas_call(
            functools.partial(kernel, n_ep, n_tp, experts),
            out_shape=jax.ShapeDtypeStruct((T, Dt), BF16),
            in_specs=[vmem] * 4 + [hbm] * 6 + [vmem],
            out_specs=vmem,
            scratch_shapes=[
                pltpu.VMEM((D, F), BF16),
                pltpu.VMEM((D, F), BF16),
                pltpu.VMEM((F, D), BF16),
                pltpu.VMEM((D, S), BF16),
                pltpu.VMEM((D, S), BF16),
                pltpu.VMEM((S, D), BF16),
                pltpu.VMEM((nz, 2, T, D + pad), BF16),
                pltpu.VMEM((2, T, F), BF16),
                pltpu.VMEM((T, S), BF16),
                pltpu.VMEM((T, D), F32),
                pltpu.VMEM((n_tp, nz, T, Dt), BF16),
                pltpu.VMEM((n_tp, nz, T, Dt), BF16),
                pltpu.VMEM((n_tp, nz, T, Dt), BF16),
                pltpu.VMEM((n_tp, nz, T, Dt), BF16),
                pltpu.VMEM((n_tp, nz, T, Dt), F32),
                pltpu.VMEM((nz, T, Dt), BF16),
                pltpu.VMEM((nz, T, Dt), BF16),
                pltpu.VMEM((T, 128), F32),
                pltpu.VMEM((n_tp, T, 128), F32),
                dma((6,)),
                dma((nz,)), dma((nz,)), dma((nz,)), dma((nz,)),
                dma((n_tp, nz)), dma((n_tp, nz)),
                dma((n_tp, nz)), dma((n_tp, nz)),
                dma((nz,)), dma((nz,)),
                dma((n_tp,)), dma((n_tp,)),
            ],
            compiler_params=pltpu.CompilerParams(collective_id=0, has_side_effects=True),
        )(
            tokens, routes.T, gates.T, norm_gain, exp_gate, exp_up, exp_down,
            sh_gate, sh_up, sh_down, out_gain,
        )

    placed = (
        P(("grp", "ep"), None),
        P(("grp", "ep"), None),
        P(("grp", "ep"), None),
        P(),
        P("ep", None, "tp"),
        P("ep", None, "tp"),
        P("ep", "tp", None),
        P(None, "tp"),
        P(None, "tp"),
        P("tp", None),
        P("tp"),
    )
    return jax.shard_map(
        shards, mesh=mesh, in_specs=placed, out_specs=P(("grp", "ep"), "tp"), check_vma=False
    )
```

time: 39.3 us -> 43.1 us (1.097)
  Pallas kernels: 37.7 us -> 41.4 us
    pallas_call x1, Pallas kernels: 37.7 us -> 41.4 us  [shards(): pl.pallas_call(functools.partial(kernel, n_ep, n_tp, experts), out_shape=...]
where the time goes in v1:
time: 43.1 us; the launch traced here: 42.9 us
  Pallas kernels  41.4 us (96%)
  local copies, waits for them, and re-layouts  1.47 us (3%)
    pallas_call x1, Pallas kernels, shards(): pl.pallas_call(functools.partial(kernel, n_ep, n_tp, experts), out_shape=...  41.4 us
    unnamed x1, local copies, waits for them, and re-layouts  1.47 us

profile of v1, /device:TPU:0, one launch (start us, length us, event | category | flops | bytes accessed | tf_op | source)
XLA Modules:
  0.0 42.9 jit_solution(13297469967122239325)
XLA Ops:
  0.0 41.4 %shard_map.109 = bf16[32,1024]{1,0:T(8,128)(2,1)} custom-call(bf16[32,2048]{1,0:T(8,128)(2,1)} %tok_ref.1, s32[4,32]{1,0:T(4,128)} %bitcast.2, f32[4,32]{1,0:T(4,128)} %bitcast.3, bf16[2048]{0:T(1024)(128)(2,1)} %ngain_ref.1, bf16[1,2048,1024]{2,1,0:T(8,128)(2,1)} %wg_hbm.1, bf16[1,2048,1024]{2,1,0:T(8,128)(2,1)} %wu_hbm.1, bf16[1,1024,2048]{2,1,0:T(8,128)(2,1)} %wd_hbm.1, ...), custom_call_target="tpu_custom_call" | custom-call | tf_op jit(solution)/shard_map/pallas_call | solution.py:244
  41.4 1.5 %copy.13 = bf16[32,1024]{1,0:T(8,128)(2,1)} copy(bf16[32,1024]{1,0:T(8,128)(2,1)} %shard_map.109) | data formatting | bytes 131072

commit v2 on v1

v2 whole, which is shorter than its diff:
```python
import functools

import jax
import jax.numpy as jnp
from jax import lax
from jax.experimental import pallas as pl
from jax.experimental.pallas import tpu as pltpu
from jax.sharding import PartitionSpec as P

EPSILON = 1e-06
MESH = pl.DeviceIdType.MESH
F32 = jnp.float32
BF16 = jnp.bfloat16


def silu(v):
    return v / (1.0 + jnp.exp(-v))


def kernel(
    n_ep, n_tp, experts,
    tok_hbm, routes_hbm, gates_hbm, ngain_hbm, wg_hbm, wu_hbm, wd_hbm, sg_hbm, su_hbm, sd_hbm, ogain_hbm,
    out_ref,
    tok, routes, gates, ngain, ogain,
    wg, wu, wd, sg, su, sd, xs, hid, shid, shp, d_out, d_in, x_out, x_in, acc, z_out, z_in, q_out, q_in,
    i_sem, w_sem, disp_send, disp_recv, pad_send, pad_recv, part_send, part_recv, fwd_send, fwd_recv,
    d_send, d_recv, x_send, x_recv, z_send, z_recv, q_send, q_recv,
):
    nz = n_ep // 2
    me = lax.axis_index("ep")
    t = lax.axis_index("tp")
    z, c = me // 2, lax.rem(me, 2)
    other = 1 - c
    T, D = tok.shape
    F = wg.shape[1]
    S = sg.shape[1]
    Dt = D // n_tp
    rows = nz * T
    pad = xs.shape[3] - D
    partner = {"ep": z * 2 + other}
    ks = list(range(1, nz))
    js = list(range(1, n_tp)) + [0]

    def tpeer(j):
        return lax.rem(t + j, n_tp)

    paired = jnp.minimum(z, nz - 1 - z)

    def distance(k):
        return jnp.where(k <= 2 * paired, (k + 1) // 2, k - paired)

    def source(k):
        if k == 0:
            return z
        to_left = jnp.where(k <= 2 * paired, k % 2 == 1, z > paired)
        return jnp.where(to_left, z - distance(k), z + distance(k))

    def seen(k):
        d, there = distance(k), source(k)
        rim = jnp.minimum(there, nz - 1 - there)
        return jnp.where(d > rim, d + rim, jnp.where(there > z, 2 * d - 1, 2 * d))

    def split(k):
        return 2 * distance(k) > nz

    barrier = pltpu.get_barrier_semaphore()
    peers = [{"ep": source(k) * 2 + c} for k in ks] + [partner] + [{"tp": tpeer(j)} for j in range(1, n_tp)]
    for peer in peers:
        pl.semaphore_signal(barrier, inc=1, device_id=peer, device_id_type=MESH)

    def load(pairs, sems):
        copies = []
        for i, (a, b) in enumerate(pairs):
            copy = pltpu.make_async_copy(a, b, sems.at[i])
            copy.start()
            copies.append(copy)
        return copies

    inputs = load(
        ((tok_hbm, tok), (ngain_hbm, ngain), (routes_hbm, routes), (gates_hbm, gates), (ogain_hbm, ogain)), i_sem
    )
    for copy in inputs:
        copy.wait()
    loads = load(
        ((wg_hbm.at[0], wg), (wu_hbm.at[0], wu), (wd_hbm.at[0], wd), (sg_hbm, sg), (su_hbm, su), (sd_hbm, sd)), w_sem
    )

    def remote(a, b, ssem, rsem, device):
        return pltpu.make_async_remote_copy(
            src_ref=a, dst_ref=b, send_sem=ssem, recv_sem=rsem, device_id=device, device_id_type=MESH
        )

    sent = []

    def send(a, b, ssem, rsem, device):
        copy = remote(a, b, ssem, rsem, device)
        copy.start()
        sent.append(copy)

    values = tok[...].astype(F32)
    scale = lax.rsqrt(jnp.mean(values * values, axis=1, keepdims=True) + EPSILON)
    xs[c, 0, :, :D] = (values * scale * ngain[...].astype(F32).reshape(1, D)).astype(BF16)
    row = lax.broadcasted_iota(jnp.int32, (pad, T), 0)
    row_expert = lax.rem(row, experts)
    dense = jnp.zeros((pad, T), F32)
    for k in range(routes.shape[0]):
        dense = dense + jnp.where(row_expert == routes[k : k + 1, :], gates[k : k + 1, :], 0.0)
    high = dense.astype(BF16).astype(F32)
    rest = dense - high
    mid = rest.astype(BF16).astype(F32)
    part = row // experts
    packed = jnp.where(part == 0, high, jnp.where(part == 1, mid, jnp.where(part == 2, rest - mid, 0.0)))
    xs[c, 0, :, D:] = packed.T.astype(BF16)

    pl.semaphore_wait(barrier, len(peers))

    own = xs.at[c, 0]

    def pad_of(k):
        return xs.at[c, k, :, pl.ds(D, pad)]

    def part_of(k, owner):
        return xs.at[c, k, :, pl.ds(pl.multiple_of(owner * Dt, Dt), Dt)]

    def dispatch(k, wanted):
        device = {"ep": source(k) * 2 + c}
        slot = seen(k)

        @pl.when(wanted & split(k))
        def _():
            remote(part_of(0, t), part_of(slot, t), part_send.at[0, k], part_recv.at[0, slot], device).start()
            remote(pad_of(0), pad_of(slot), pad_send.at[k], pad_recv.at[slot], device).start()

        @pl.when(wanted & ~split(k))
        def _():
            remote(own, xs.at[c, slot], disp_send.at[k], disp_recv.at[slot], device).start()

    for k in ks[:2]:
        dispatch(k, distance(k) == 1)
    for k in ks[::-1]:
        dispatch(k, distance(k) > 1)
    send(own, own, fwd_send.at[0], fwd_recv.at[0], partner)

    dtile = min(512, Dt)

    def shared():
        loads[3].wait()
        loads[4].wait()
        tile = min(256, S)

        @pl.loop(0, S // tile)
        def _(i):
            cols = pl.ds(pl.multiple_of(i * tile, tile), tile)
            x = xs[c, 0, :, :D]
            g = jnp.dot(x, sg[:, cols], preferred_element_type=F32)
            u = jnp.dot(x, su[:, cols], preferred_element_type=F32)
            shid[:, cols] = (silu(g) * u).astype(BF16)

        loads[5].wait()

        @pl.loop(0, D // dtile)
        def _(i):
            cols = pl.ds(pl.multiple_of(i * dtile, dtile), dtile)
            shp[:, cols] = jnp.dot(shid[...], sd[:, cols], preferred_element_type=F32)

    def relay(k):
        @pl.when(split(k))
        def _():
            piece = part_of(k, t)
            remote(piece, piece, part_send.at[0, k], part_recv.at[0, k], partner).wait_recv()
            for j in range(1, n_tp):
                remote(piece, piece, part_send.at[j, k], part_recv.at[j, k], {"tp": tpeer(j)}).start()

    def forward(k):
        return remote(xs.at[c, k], xs.at[c, k], fwd_send.at[k], fwd_recv.at[k], partner)

    def arrive(k):
        @pl.when(split(k))
        def _():
            remote(pad_of(k), pad_of(k), pad_send.at[k], pad_recv.at[k], partner).wait_recv()
            for j in range(1, n_tp):
                piece = part_of(k, lax.rem(t - j + n_tp, n_tp))
                remote(piece, piece, part_send.at[j, k], part_recv.at[j, k], partner).wait_recv()

        @pl.when(~split(k))
        def _():
            block = xs.at[c, k]
            remote(block, block, disp_send.at[k], disp_recv.at[k], partner).wait_recv()

        forward(k).start()

    def swap(k):
        block = xs.at[other, k]
        remote(block, block, fwd_send.at[k], fwd_recv.at[k], partner).wait_recv()

    ftile = min(512, F)

    glane = lax.broadcasted_iota(jnp.int32, (rows, pad), 1)
    mine = (lax.rem(glane, experts) == me) & (glane < 3 * experts)

    def hidden(half):
        packed_gates = xs[half, :, :, D:].reshape(rows, pad).astype(F32)
        weight = jnp.sum(jnp.where(mine, packed_gates, 0.0), axis=1, keepdims=True)
        for i in range(F // ftile):
            cols = pl.ds(i * ftile, ftile)
            x = xs[half, :, :, :D].reshape(rows, D)
            g = jnp.dot(x, wg[:, cols], preferred_element_type=F32)
            u = jnp.dot(x, wu[:, cols], preferred_element_type=F32)
            hid[half, :, cols] = (silu(g) * u * weight).astype(BF16)

    tiles = list(range(Dt // dtile))

    def columns(j, i):
        return pl.ds(pl.multiple_of(tpeer(j) * Dt + i * dtile, dtile), dtile)

    def down(half, j, i):
        return jnp.dot(hid[half], wd[:, columns(j, i)], preferred_element_type=F32).reshape(nz, T, dtile)

    def pass_over(j, i, k):
        return remote(d_out.at[j, i, k], d_in.at[j, i, k], d_send.at[j, i, k], d_recv.at[j, i, k], partner)

    def give(j):
        for i in tiles:
            d_out[j, i] = down(other, j, i).astype(BF16)
            for k in range(nz):
                copy = pass_over(j, i, k)
                copy.start()
                sent.append(copy)

    def keep(j):
        for i in tiles:
            acc[j, i] = down(c, j, i)

    def cross(j, i, k):
        return remote(x_out.at[j, i, k], x_in.at[j, i, k], x_send.at[j, i, k], x_recv.at[j, i, k], {"tp": tpeer(j)})

    def pair(j, k):
        for i in tiles:
            pass_over(j, i, k).wait_recv()
            total = acc[j, i, k] + d_in[j, i, k].astype(F32)
            if k == 0:
                total = total + shp[:, columns(j, i)]
            if j == 0:
                acc[0, i, k] = total
            else:
                x_out[j, i, k] = total.astype(BF16)
                copy = cross(j, i, k)
                copy.start()
                sent.append(copy)

    def finish(k):
        for i in tiles:
            total = acc[0, i, k]
            for j in range(1, n_tp):
                cross(j, i, k).wait_recv()
                total = total + x_in[j, i, k].astype(F32)
            if k == 0:
                acc[0, i, k] = total
            else:
                z_out[k, :, i * dtile : (i + 1) * dtile] = total.astype(BF16)
        if k:
            slot = seen(k)
            send(z_out.at[k], z_in.at[slot], z_send.at[k], z_recv.at[slot], {"ep": source(k) * 2 + c})

    for k in ks[:1]:
        arrive(k)
    for k in ks:
        relay(k)
    for k in ks[1:]:
        arrive(k)
    for copy in loads[:2]:
        copy.wait()
    hidden(c)
    for k in [0] + ks:
        swap(k)
    hidden(other)
    loads[2].wait()
    far_first = ks[::-1]
    for n, j in enumerate(js):
        give(j)
        if n:
            for k in far_first:
                pair(js[n - 1], k)
        keep(j)
    for k in far_first:
        pair(js[-1], k)
    shared()
    for j in js:
        pair(j, 0)
    for k in far_first + [0]:
        finish(k)

    total = jnp.concatenate([acc[0, i, 0] for i in tiles], axis=1)
    for k in ks:
        remote(z_out.at[k], z_in.at[k], z_send.at[k], z_recv.at[k], partner).wait_recv()
        total = total + z_in[k].astype(F32)
    squares = jnp.sum(total * total, axis=1, keepdims=True)
    q_out[...] = jnp.broadcast_to(squares, q_out.shape)
    for j in range(1, n_tp):
        send(q_out, q_in.at[j], q_send.at[j], q_recv.at[j], {"tp": tpeer(j)})
    gained = total * ogain[...].astype(F32).reshape(1, Dt)
    for j in range(1, n_tp):
        remote(q_out, q_in.at[j], q_send.at[j], q_recv.at[j], partner).wait_recv()
        squares = squares + q_in[j, :, :1]
    out_ref[...] = (gained * lax.rsqrt(squares / D + EPSILON)).astype(BF16)

    for copy in sent:
        copy.wait_send()
    for k in ks:
        forward(k).wait_send()

        @pl.when(split(k))
        def _():
            remote(pad_of(0), pad_of(k), pad_send.at[k], pad_recv.at[k], partner).wait_send()
            for j in range(n_tp):
                remote(part_of(0, t), part_of(k, t), part_send.at[j, k], part_recv.at[j, k], partner).wait_send()

        @pl.when(~split(k))
        def _():
            remote(own, xs.at[c, k], disp_send.at[k], disp_recv.at[k], partner).wait_send()


def solution(mesh):
    n_ep, n_tp = mesh.shape["ep"], mesh.shape["tp"]
    nz = n_ep // 2

    def shards(tokens, routes, gates, norm_gain, exp_gate, exp_up, exp_down, sh_gate, sh_up, sh_down, out_gain):
        T, D = tokens.shape
        local, _, F = exp_gate.shape
        S = sh_gate.shape[1]
        assert local == 1
        experts = local * n_ep
        Dt = D // n_tp
        pad = 128 * ((3 * experts + 127) // 128)
        dtile = min(512, Dt)
        tiles = Dt // dtile
        vmem = pl.BlockSpec(memory_space=pltpu.VMEM)
        hbm = pl.BlockSpec(memory_space=pl.ANY)
        dma = pltpu.SemaphoreType.DMA
        return pl.pallas_call(
            functools.partial(kernel, n_ep, n_tp, experts),
            out_shape=jax.ShapeDtypeStruct((T, Dt), BF16),
            in_specs=[hbm] * 11,
            out_specs=vmem,
            scratch_shapes=[
                pltpu.VMEM(tokens.shape, BF16),
                pltpu.VMEM(routes.shape[::-1], jnp.int32),
                pltpu.VMEM(gates.shape[::-1], F32),
                pltpu.VMEM(norm_gain.shape, BF16),
                pltpu.VMEM(out_gain.shape, BF16),
                pltpu.VMEM((D, F), BF16),
                pltpu.VMEM((D, F), BF16),
                pltpu.VMEM((F, D), BF16),
                pltpu.VMEM((D, S), BF16),
                pltpu.VMEM((D, S), BF16),
                pltpu.VMEM((S, D), BF16),
                pltpu.VMEM((2, nz, T, D + pad), BF16),
                pltpu.VMEM((2, nz * T, F), BF16),
                pltpu.VMEM((T, S), BF16),
                pltpu.VMEM((T, D), F32),
                pltpu.VMEM((n_tp, tiles, nz, T, dtile), BF16),
                pltpu.VMEM((n_tp, tiles, nz, T, dtile), BF16),
                pltpu.VMEM((n_tp, tiles, nz, T, dtile), BF16),
                pltpu.VMEM((n_tp, tiles, nz, T, dtile), BF16),
                pltpu.VMEM((n_tp, tiles, nz, T, dtile), F32),
                pltpu.VMEM((nz, T, Dt), BF16),
                pltpu.VMEM((nz, T, Dt), BF16),
                pltpu.VMEM((T, 128), F32),
                pltpu.VMEM((n_tp, T, 128), F32),
                dma((5,)), dma((6,)),
                dma((nz,)), dma((nz,)), dma((nz,)), dma((nz,)),
                dma((n_tp, nz)), dma((n_tp, nz)),
                dma((nz,)), dma((nz,)),
                dma((n_tp, tiles, nz)), dma((n_tp, tiles, nz)),
                dma((n_tp, tiles, nz)), dma((n_tp, tiles, nz)),
                dma((nz,)), dma((nz,)),
                dma((n_tp,)), dma((n_tp,)),
            ],
            compiler_params=pltpu.CompilerParams(collective_id=0, has_side_effects=True),
        )(
            tokens, routes.T, gates.T, norm_gain, exp_gate, exp_up, exp_down,
            sh_gate, sh_up, sh_down, out_gain,
        )

    placed = (
        P(("grp", "ep"), None),
        P(("grp", "ep"), None),
        P(("grp", "ep"), None),
        P(),
        P("ep", None, "tp"),
        P("ep", None, "tp"),
        P("ep", "tp", None),
        P(None, "tp"),
        P(None, "tp"),
        P("tp", None),
        P("tp"),
    )
    return jax.shard_map(
        shards, mesh=mesh, in_specs=placed, out_specs=P(("grp", "ep"), "tp"), check_vma=False
    )
```

time: 43.1 us -> 36.4 us (0.84)
  Pallas kernels: 41.4 us -> 34.8 us
    pallas_call x1, Pallas kernels: 41.4 us -> 34.8 us  [shards(): pl.pallas_call(functools.partial(kernel, n_ep, n_tp, experts), out_shape=...]
where the time goes in v2:
time: 36.4 us; the launch traced here: 36.3 us
  Pallas kernels  34.8 us (96%)
  local copies, waits for them, and re-layouts  1.47 us (4%)
    pallas_call x1, Pallas kernels, shards(): pl.pallas_call(functools.partial(kernel, n_ep, n_tp, experts), out_shape=...  34.8 us
    unnamed x1, local copies, waits for them, and re-layouts  1.47 us

profile of v2, /device:TPU:0, one launch (start us, length us, event | category | flops | bytes accessed | tf_op | source)
XLA Modules:
  0.0 36.3 jit_solution(8718030386952218464)
XLA Ops:
  0.0 34.8 %shard_map.109 = bf16[32,1024]{1,0:T(8,128)(2,1)} custom-call(bf16[32,2048]{1,0:T(8,128)(2,1)} %tok_hbm.1, s32[4,32]{1,0:T(4,128)} %bitcast.2, f32[4,32]{1,0:T(4,128)} %bitcast.3, bf16[2048]{0:T(1024)(128)(2,1)} %ngain_hbm.1, bf16[1,2048,1024]{2,1,0:T(8,128)(2,1)} %wg_hbm.1, bf16[1,2048,1024]{2,1,0:T(8,128)(2,1)} %wu_hbm.1, bf16[1,1024,2048]{2,1,0:T(8,128)(2,1)} %wd_hbm.1, ...), custom_call_target="tpu_custom_call" | custom-call | tf_op jit(solution)/shard_map/pallas_call | solution.py:340
  34.8 1.5 %copy.13 = bf16[32,1024]{1,0:T(8,128)(2,1)} copy(bf16[32,1024]{1,0:T(8,128)(2,1)} %shard_map.109) | data formatting | bytes 131072

commit v3 on v2

--- a/solution.py
+++ b/solution.py
@@ -52,16 +52,24 @@
     def source(k):
         if k == 0:
             return z
-        to_left = jnp.where(k <= 2 * paired, k % 2 == 1, z > paired)
+        low = 2 * z < nz
+        to_left = jnp.where(k <= 2 * paired, low if k % 2 else ~low, z > paired)
         return jnp.where(to_left, z - distance(k), z + distance(k))
 
     def seen(k):
         d, there = distance(k), source(k)
         rim = jnp.minimum(there, nz - 1 - there)
-        return jnp.where(d > rim, d + rim, jnp.where(there > z, 2 * d - 1, 2 * d))
-
-    def split(k):
-        return 2 * distance(k) > nz
+        outer = jnp.where(2 * there < nz, z < there, z > there)
+        return jnp.where(d > rim, d + rim, jnp.where(outer, 2 * d - 1, 2 * d))
+
+    def mirror(k):
+        return source(k) + z == nz - 1
+
+    def beyond(k):
+        return ((2 * source(k) < nz) != (2 * z < nz)) & ~mirror(k)
+
+    def near(k):
+        return (2 * source(k) < nz) == (2 * z < nz)
 
     barrier = pltpu.get_barrier_semaphore()
     peers = [{"ep": source(k) * 2 + c} for k in ks] + [partner] + [{"tp": tpeer(j)} for j in range(1, n_tp)]
@@ -79,7 +87,7 @@
     inputs = load(
         ((tok_hbm, tok), (ngain_hbm, ngain), (routes_hbm, routes), (gates_hbm, gates), (ogain_hbm, ogain)), i_sem
     )
-    for copy in inputs:
+    for copy in inputs[:2]:
         copy.wait()
     loads = load(
         ((wg_hbm.at[0], wg), (wu_hbm.at[0], wu), (wd_hbm.at[0], wd), (sg_hbm, sg), (su_hbm, su), (sd_hbm, sd)), w_sem
@@ -100,6 +108,52 @@
     values = tok[...].astype(F32)
     scale = lax.rsqrt(jnp.mean(values * values, axis=1, keepdims=True) + EPSILON)
     xs[c, 0, :, :D] = (values * scale * ngain[...].astype(F32).reshape(1, D)).astype(BF16)
+    pl.semaphore_wait(barrier, len(peers))
+
+    own = xs.at[c, 0]
+
+    def pad_of(k):
+        return xs.at[c, k, :, pl.ds(D, pad)]
+
+    def part_of(k, owner):
+        return xs.at[c, k, :, pl.ds(pl.multiple_of(owner * Dt, Dt), Dt)]
+
+    def half_of(k, owner):
+        return xs.at[c, k, :, pl.ds(pl.multiple_of(owner * (Dt // 2), Dt // 2), Dt // 2)]
+
+    def rest_of(k):
+        return xs.at[c, k, :, pl.ds(D // 2, D // 2 + pad)]
+
+    def first_pieces(k):
+        device, slot = {"ep": source(k) * 2 + c}, seen(k)
+
+        @pl.when(mirror(k))
+        def _():
+            remote(part_of(0, t), part_of(slot, t), part_send.at[0, k], part_recv.at[0, slot], device).start()
+
+        @pl.when(beyond(k))
+        def _():
+            remote(half_of(0, t), half_of(slot, t), part_send.at[0, k], part_recv.at[0, slot], device).start()
+
+    def whole(k):
+        device, slot = {"ep": source(k) * 2 + c}, seen(k)
+
+        @pl.when(mirror(k))
+        def _():
+            remote(pad_of(0), pad_of(slot), pad_send.at[k], pad_recv.at[slot], device).start()
+
+        @pl.when(near(k))
+        def _():
+            remote(own, xs.at[c, slot], disp_send.at[k], disp_recv.at[slot], device).start()
+
+        @pl.when(beyond(k))
+        def _():
+            remote(rest_of(0), rest_of(slot), disp_send.at[k], disp_recv.at[slot], device).start()
+
+    for k in ks:
+        first_pieces(k)
+    for copy in inputs[2:]:
+        copy.wait()
     row = lax.broadcasted_iota(jnp.int32, (pad, T), 0)
     row_expert = lax.rem(row, experts)
     dense = jnp.zeros((pad, T), F32)
@@ -112,33 +166,8 @@
     packed = jnp.where(part == 0, high, jnp.where(part == 1, mid, jnp.where(part == 2, rest - mid, 0.0)))
     xs[c, 0, :, D:] = packed.T.astype(BF16)
 
-    pl.semaphore_wait(barrier, len(peers))
-
-    own = xs.at[c, 0]
-
-    def pad_of(k):
-        return xs.at[c, k, :, pl.ds(D, pad)]
-
-    def part_of(k, owner):
-        return xs.at[c, k, :, pl.ds(pl.multiple_of(owner * Dt, Dt), Dt)]
-
-    def dispatch(k, wanted):
-        device = {"ep": source(k) * 2 + c}
-        slot = seen(k)
-
-        @pl.when(wanted & split(k))
-        def _():
-            remote(part_of(0, t), part_of(slot, t), part_send.at[0, k], part_recv.at[0, slot], device).start()
-            remote(pad_of(0), pad_of(slot), pad_send.at[k], pad_recv.at[slot], device).start()
-
-        @pl.when(wanted & ~split(k))
-        def _():
-            remote(own, xs.at[c, slot], disp_send.at[k], disp_recv.at[slot], device).start()
-
-    for k in ks[:2]:
-        dispatch(k, distance(k) == 1)
-    for k in ks[::-1]:
-        dispatch(k, distance(k) > 1)
+    for k in ks:
+        whole(k)
     send(own, own, fwd_send.at[0], fwd_recv.at[0], partner)
 
     dtile = min(512, Dt)
@@ -164,25 +193,35 @@
             shp[:, cols] = jnp.dot(shid[...], sd[:, cols], preferred_element_type=F32)
 
     def relay(k):
-        @pl.when(split(k))
-        def _():
-            piece = part_of(k, t)
+        def go(of):
+            piece = of(k, t)
             remote(piece, piece, part_send.at[0, k], part_recv.at[0, k], partner).wait_recv()
             for j in range(1, n_tp):
                 remote(piece, piece, part_send.at[j, k], part_recv.at[j, k], {"tp": tpeer(j)}).start()
 
+        pl.when(mirror(k))(lambda: go(part_of))
+        pl.when(beyond(k))(lambda: go(half_of))
+
     def forward(k):
         return remote(xs.at[c, k], xs.at[c, k], fwd_send.at[k], fwd_recv.at[k], partner)
 
     def arrive(k):
-        @pl.when(split(k))
+        def go(of):
+            for j in range(1, n_tp):
+                piece = of(k, lax.rem(t - j + n_tp, n_tp))
+                remote(piece, piece, part_send.at[j, k], part_recv.at[j, k], partner).wait_recv()
+
+        @pl.when(mirror(k))
         def _():
             remote(pad_of(k), pad_of(k), pad_send.at[k], pad_recv.at[k], partner).wait_recv()
-            for j in range(1, n_tp):
-                piece = part_of(k, lax.rem(t - j + n_tp, n_tp))
-                remote(piece, piece, part_send.at[j, k], part_recv.at[j, k], partner).wait_recv()
-
-        @pl.when(~split(k))
+            go(part_of)
+
+        @pl.when(beyond(k))
+        def _():
+            go(half_of)
+            remote(rest_of(k), rest_of(k), disp_send.at[k], disp_recv.at[k], partner).wait_recv()
+
+        @pl.when(near(k))
         def _():
             block = xs.at[c, k]
             remote(block, block, disp_send.at[k], disp_recv.at[k], partner).wait_recv()
@@ -257,16 +296,15 @@
             if k == 0:
                 acc[0, i, k] = total
             else:
-                z_out[k, :, i * dtile : (i + 1) * dtile] = total.astype(BF16)
-        if k:
-            slot = seen(k)
-            send(z_out.at[k], z_in.at[slot], z_send.at[k], z_recv.at[slot], {"ep": source(k) * 2 + c})
-
-    for k in ks[:1]:
-        arrive(k)
+                z_out[i, k] = total.astype(BF16)
+                slot = seen(k)
+                send(
+                    z_out.at[i, k], z_in.at[i, slot], z_send.at[i, k], z_recv.at[i, slot], {"ep": source(k) * 2 + c}
+                )
+
     for k in ks:
         relay(k)
-    for k in ks[1:]:
+    for k in ks:
         arrive(k)
     for copy in loads[:2]:
         copy.wait()
@@ -290,10 +328,12 @@
     for k in far_first + [0]:
         finish(k)
 
-    total = jnp.concatenate([acc[0, i, 0] for i in tiles], axis=1)
-    for k in ks:
-        remote(z_out.at[k], z_in.at[k], z_send.at[k], z_recv.at[k], partner).wait_recv()
-        total = total + z_in[k].astype(F32)
+    totals = [acc[0, i, 0] for i in tiles]
+    for k in ks:
+        for i in tiles:
+            remote(z_out.at[i, k], z_in.at[i, k], z_send.at[i, k], z_recv.at[i, k], partner).wait_recv()
+            totals[i] = totals[i] + z_in[i, k].astype(F32)
+    total = jnp.concatenate(totals, axis=1)
     squares = jnp.sum(total * total, axis=1, keepdims=True)
     q_out[...] = jnp.broadcast_to(squares, q_out.shape)
     for j in range(1, n_tp):
@@ -309,13 +349,19 @@
     for k in ks:
         forward(k).wait_send()
 
-        @pl.when(split(k))
+        @pl.when(mirror(k))
         def _():
             remote(pad_of(0), pad_of(k), pad_send.at[k], pad_recv.at[k], partner).wait_send()
             for j in range(n_tp):
                 remote(part_of(0, t), part_of(k, t), part_send.at[j, k], part_recv.at[j, k], partner).wait_send()
 
-        @pl.when(~split(k))
+        @pl.when(beyond(k))
+        def _():
+            for j in range(n_tp):
+                remote(half_of(0, t), half_of(k, t), part_send.at[j, k], part_recv.at[j, k], partner).wait_send()
+            remote(rest_of(0), rest_of(k), disp_send.at[k], disp_recv.at[k], partner).wait_send()
+
+        @pl.when(near(k))
         def _():
             remote(own, xs.at[c, k], disp_send.at[k], disp_recv.at[k], partner).wait_send()
 
@@ -363,8 +409,8 @@
                 pltpu.VMEM((n_tp, tiles, nz, T, dtile), BF16),
                 pltpu.VMEM((n_tp, tiles, nz, T, dtile), BF16),
                 pltpu.VMEM((n_tp, tiles, nz, T, dtile), F32),
-                pltpu.VMEM((nz, T, Dt), BF16),
-                pltpu.VMEM((nz, T, Dt), BF16),
+                pltpu.VMEM((tiles, nz, T, dtile), BF16),
+                pltpu.VMEM((tiles, nz, T, dtile), BF16),
                 pltpu.VMEM((T, 128), F32),
                 pltpu.VMEM((n_tp, T, 128), F32),
                 dma((5,)), dma((6,)),
@@ -373,7 +419,7 @@
                 dma((nz,)), dma((nz,)),
                 dma((n_tp, tiles, nz)), dma((n_tp, tiles, nz)),
                 dma((n_tp, tiles, nz)), dma((n_tp, tiles, nz)),
-                dma((nz,)), dma((nz,)),
+                dma((tiles, nz)), dma((tiles, nz)),
                 dma((n_tp,)), dma((n_tp,)),
             ],
             compiler_params=pltpu.CompilerParams(collective_id=0, has_side_effects=True),

time: 36.4 us -> 35.2 us (0.967)
  Pallas kernels: 34.8 us -> 33.6 us
    pallas_call x1, Pallas kernels: 34.8 us -> 33.6 us  [shards(): pl.pallas_call(functools.partial(kernel, n_ep, n_tp, experts), out_shape=...]
where the time goes in v3:
time: 35.2 us; the launch traced here: 35.1 us
  Pallas kernels  33.6 us (95%)
  local copies, waits for them, and re-layouts  1.47 us (4%)
    pallas_call x1, Pallas kernels, shards(): pl.pallas_call(functools.partial(kernel, n_ep, n_tp, experts), out_shape=...  33.6 us
    unnamed x1, local copies, waits for them, and re-layouts  1.47 us

profile of v3, /device:TPU:0, one launch (start us, length us, event | category | flops | bytes accessed | tf_op | source)
XLA Modules:
  0.0 35.1 jit_solution(13974661101134138962)
XLA Ops:
  0.0 33.6 %shard_map.109 = bf16[32,1024]{1,0:T(8,128)(2,1)} custom-call(bf16[32,2048]{1,0:T(8,128)(2,1)} %tok_hbm.1, s32[4,32]{1,0:T(4,128)} %bitcast.2, f32[4,32]{1,0:T(4,128)} %bitcast.3, bf16[2048]{0:T(1024)(128)(2,1)} %ngain_hbm.1, bf16[1,2048,1024]{2,1,0:T(8,128)(2,1)} %wg_hbm.1, bf16[1,2048,1024]{2,1,0:T(8,128)(2,1)} %wu_hbm.1, bf16[1,1024,2048]{2,1,0:T(8,128)(2,1)} %wd_hbm.1, ...), custom_call_target="tpu_custom_call" | custom-call | tf_op jit(solution)/shard_map/pallas_call | solution.py:386
  33.6 1.5 %copy.13 = bf16[32,1024]{1,0:T(8,128)(2,1)} copy(bf16[32,1024]{1,0:T(8,128)(2,1)} %shard_map.109) | data formatting | bytes 131072

commit v4 on v3

--- a/solution.py
+++ b/solution.py
@@ -23,7 +23,7 @@
     out_ref,
     tok, routes, gates, ngain, ogain,
     wg, wu, wd, sg, su, sd, xs, hid, shid, shp, d_out, d_in, x_out, x_in, acc, z_out, z_in, q_out, q_in,
-    i_sem, w_sem, disp_send, disp_recv, pad_send, pad_recv, part_send, part_recv, fwd_send, fwd_recv,
+    i_sem, w_sem, disp_send, disp_recv, part_send, part_recv, fwd_send, fwd_recv,
     d_send, d_recv, x_send, x_recv, z_send, z_recv, q_send, q_recv,
 ):
     nz = n_ep // 2
@@ -62,14 +62,8 @@
         outer = jnp.where(2 * there < nz, z < there, z > there)
         return jnp.where(d > rim, d + rim, jnp.where(outer, 2 * d - 1, 2 * d))
 
-    def mirror(k):
-        return source(k) + z == nz - 1
-
     def beyond(k):
-        return ((2 * source(k) < nz) != (2 * z < nz)) & ~mirror(k)
-
-    def near(k):
-        return (2 * source(k) < nz) == (2 * z < nz)
+        return (2 * source(k) < nz) != (2 * z < nz)
 
     barrier = pltpu.get_barrier_semaphore()
     peers = [{"ep": source(k) * 2 + c} for k in ks] + [partner] + [{"tp": tpeer(j)} for j in range(1, n_tp)]
@@ -112,12 +106,6 @@
 
     own = xs.at[c, 0]
 
-    def pad_of(k):
-        return xs.at[c, k, :, pl.ds(D, pad)]
-
-    def part_of(k, owner):
-        return xs.at[c, k, :, pl.ds(pl.multiple_of(owner * Dt, Dt), Dt)]
-
     def half_of(k, owner):
         return xs.at[c, k, :, pl.ds(pl.multiple_of(owner * (Dt // 2), Dt // 2), Dt // 2)]
 
@@ -127,10 +115,6 @@
     def first_pieces(k):
         device, slot = {"ep": source(k) * 2 + c}, seen(k)
 
-        @pl.when(mirror(k))
-        def _():
-            remote(part_of(0, t), part_of(slot, t), part_send.at[0, k], part_recv.at[0, slot], device).start()
-
         @pl.when(beyond(k))
         def _():
             remote(half_of(0, t), half_of(slot, t), part_send.at[0, k], part_recv.at[0, slot], device).start()
@@ -138,11 +122,7 @@
     def whole(k):
         device, slot = {"ep": source(k) * 2 + c}, seen(k)
 
-        @pl.when(mirror(k))
-        def _():
-            remote(pad_of(0), pad_of(slot), pad_send.at[k], pad_recv.at[slot], device).start()
-
-        @pl.when(near(k))
+        @pl.when(~beyond(k))
         def _():
             remote(own, xs.at[c, slot], disp_send.at[k], disp_recv.at[slot], device).start()
 
@@ -193,35 +173,25 @@
             shp[:, cols] = jnp.dot(shid[...], sd[:, cols], preferred_element_type=F32)
 
     def relay(k):
-        def go(of):
-            piece = of(k, t)
+        @pl.when(beyond(k))
+        def _():
+            piece = half_of(k, t)
             remote(piece, piece, part_send.at[0, k], part_recv.at[0, k], partner).wait_recv()
             for j in range(1, n_tp):
                 remote(piece, piece, part_send.at[j, k], part_recv.at[j, k], {"tp": tpeer(j)}).start()
 
-        pl.when(mirror(k))(lambda: go(part_of))
-        pl.when(beyond(k))(lambda: go(half_of))
-
     def forward(k):
         return remote(xs.at[c, k], xs.at[c, k], fwd_send.at[k], fwd_recv.at[k], partner)
 
     def arrive(k):
-        def go(of):
+        @pl.when(beyond(k))
+        def _():
             for j in range(1, n_tp):
-                piece = of(k, lax.rem(t - j + n_tp, n_tp))
+                piece = half_of(k, lax.rem(t - j + n_tp, n_tp))
                 remote(piece, piece, part_send.at[j, k], part_recv.at[j, k], partner).wait_recv()
-
-        @pl.when(mirror(k))
-        def _():
-            remote(pad_of(k), pad_of(k), pad_send.at[k], pad_recv.at[k], partner).wait_recv()
-            go(part_of)
-
-        @pl.when(beyond(k))
-        def _():
-            go(half_of)
             remote(rest_of(k), rest_of(k), disp_send.at[k], disp_recv.at[k], partner).wait_recv()
 
-        @pl.when(near(k))
+        @pl.when(~beyond(k))
         def _():
             block = xs.at[c, k]
             remote(block, block, disp_send.at[k], disp_recv.at[k], partner).wait_recv()
@@ -261,7 +231,7 @@
     def give(j):
         for i in tiles:
             d_out[j, i] = down(other, j, i).astype(BF16)
-            for k in range(nz):
+            for k in ks[::-1] + [0]:
                 copy = pass_over(j, i, k)
                 copy.start()
                 sent.append(copy)
@@ -349,19 +319,13 @@
     for k in ks:
         forward(k).wait_send()
 
-        @pl.when(mirror(k))
-        def _():
-            remote(pad_of(0), pad_of(k), pad_send.at[k], pad_recv.at[k], partner).wait_send()
-            for j in range(n_tp):
-                remote(part_of(0, t), part_of(k, t), part_send.at[j, k], part_recv.at[j, k], partner).wait_send()
-
         @pl.when(beyond(k))
         def _():
             for j in range(n_tp):
                 remote(half_of(0, t), half_of(k, t), part_send.at[j, k], part_recv.at[j, k], partner).wait_send()
             remote(rest_of(0), rest_of(k), disp_send.at[k], disp_recv.at[k], partner).wait_send()
 
-        @pl.when(near(k))
+        @pl.when(~beyond(k))
         def _():
             remote(own, xs.at[c, k], disp_send.at[k], disp_recv.at[k], partner).wait_send()
 
@@ -414,7 +378,7 @@
                 pltpu.VMEM((T, 128), F32),
                 pltpu.VMEM((n_tp, T, 128), F32),
                 dma((5,)), dma((6,)),
-                dma((nz,)), dma((nz,)), dma((nz,)), dma((nz,)),
+                dma((nz,)), dma((nz,)),
                 dma((n_tp, nz)), dma((n_tp, nz)),
                 dma((nz,)), dma((nz,)),
                 dma((n_tp, tiles, nz)), dma((n_tp, tiles, nz)),

time: 35.2 us -> 34.8 us (0.989)
  Pallas kernels: 33.6 us -> 33.1 us
    pallas_call x1, Pallas kernels: 33.6 us -> 33.1 us  [shards(): pl.pallas_call(functools.partial(kernel, n_ep, n_tp, experts), out_shape=...]
where the time goes in v4:
time: 34.8 us; the launch traced here: 34.6 us
  Pallas kernels  33.1 us (95%)
  local copies, waits for them, and re-layouts  1.47 us (4%)
    pallas_call x1, Pallas kernels, shards(): pl.pallas_call(functools.partial(kernel, n_ep, n_tp, experts), out_shape=...  33.1 us
    unnamed x1, local copies, waits for them, and re-layouts  1.47 us

profile of v4, /device:TPU:0, one launch (start us, length us, event | category | flops | bytes accessed | tf_op | source)
XLA Modules:
  0.0 34.6 jit_solution(5146054540428502193)
XLA Ops:
  0.0 33.1 %shard_map.109 = bf16[32,1024]{1,0:T(8,128)(2,1)} custom-call(bf16[32,2048]{1,0:T(8,128)(2,1)} %tok_hbm.1, s32[4,32]{1,0:T(4,128)} %bitcast.2, f32[4,32]{1,0:T(4,128)} %bitcast.3, bf16[2048]{0:T(1024)(128)(2,1)} %ngain_hbm.1, bf16[1,2048,1024]{2,1,0:T(8,128)(2,1)} %wg_hbm.1, bf16[1,2048,1024]{2,1,0:T(8,128)(2,1)} %wu_hbm.1, bf16[1,1024,2048]{2,1,0:T(8,128)(2,1)} %wd_hbm.1, ...), custom_call_target="tpu_custom_call" | custom-call | tf_op jit(solution)/shard_map/pallas_call | solution.py:350
  33.1 1.5 %copy.13 = bf16[32,1024]{1,0:T(8,128)(2,1)} copy(bf16[32,1024]{1,0:T(8,128)(2,1)} %shard_map.109) | data formatting | bytes 131072

commit v5 on v4

--- a/solution.py
+++ b/solution.py
@@ -102,36 +102,6 @@
     values = tok[...].astype(F32)
     scale = lax.rsqrt(jnp.mean(values * values, axis=1, keepdims=True) + EPSILON)
     xs[c, 0, :, :D] = (values * scale * ngain[...].astype(F32).reshape(1, D)).astype(BF16)
-    pl.semaphore_wait(barrier, len(peers))
-
-    own = xs.at[c, 0]
-
-    def half_of(k, owner):
-        return xs.at[c, k, :, pl.ds(pl.multiple_of(owner * (Dt // 2), Dt // 2), Dt // 2)]
-
-    def rest_of(k):
-        return xs.at[c, k, :, pl.ds(D // 2, D // 2 + pad)]
-
-    def first_pieces(k):
-        device, slot = {"ep": source(k) * 2 + c}, seen(k)
-
-        @pl.when(beyond(k))
-        def _():
-            remote(half_of(0, t), half_of(slot, t), part_send.at[0, k], part_recv.at[0, slot], device).start()
-
-    def whole(k):
-        device, slot = {"ep": source(k) * 2 + c}, seen(k)
-
-        @pl.when(~beyond(k))
-        def _():
-            remote(own, xs.at[c, slot], disp_send.at[k], disp_recv.at[slot], device).start()
-
-        @pl.when(beyond(k))
-        def _():
-            remote(rest_of(0), rest_of(slot), disp_send.at[k], disp_recv.at[slot], device).start()
-
-    for k in ks:
-        first_pieces(k)
     for copy in inputs[2:]:
         copy.wait()
     row = lax.broadcasted_iota(jnp.int32, (pad, T), 0)
@@ -146,6 +116,36 @@
     packed = jnp.where(part == 0, high, jnp.where(part == 1, mid, jnp.where(part == 2, rest - mid, 0.0)))
     xs[c, 0, :, D:] = packed.T.astype(BF16)
 
+    pl.semaphore_wait(barrier, len(peers))
+
+    own = xs.at[c, 0]
+
+    def half_of(k, owner):
+        return xs.at[c, k, :, pl.ds(pl.multiple_of(owner * (Dt // 2), Dt // 2), Dt // 2)]
+
+    def rest_of(k):
+        return xs.at[c, k, :, pl.ds(D // 2, D // 2 + pad)]
+
+    def first_pieces(k):
+        device, slot = {"ep": source(k) * 2 + c}, seen(k)
+
+        @pl.when(beyond(k))
+        def _():
+            remote(half_of(0, t), half_of(slot, t), part_send.at[0, k], part_recv.at[0, slot], device).start()
+
+    def whole(k):
+        device, slot = {"ep": source(k) * 2 + c}, seen(k)
+
+        @pl.when(~beyond(k))
+        def _():
+            remote(own, xs.at[c, slot], disp_send.at[k], disp_recv.at[slot], device).start()
+
+        @pl.when(beyond(k))
+        def _():
+            remote(rest_of(0), rest_of(slot), disp_send.at[k], disp_recv.at[slot], device).start()
+
+    for k in ks:
+        first_pieces(k)
     for k in ks:
         whole(k)
     send(own, own, fwd_send.at[0], fwd_recv.at[0], partner)

time: 34.8 us -> 34.8 us (level)
  no operation moved by 1% of the time
where the time goes in v5:
time: 34.8 us; the launch traced here: 34.6 us
  Pallas kernels  33.1 us (95%)
  local copies, waits for them, and re-layouts  1.47 us (4%)
    pallas_call x1, Pallas kernels, shards(): pl.pallas_call(functools.partial(kernel, n_ep, n_tp, experts), out_shape=...  33.1 us
    unnamed x1, local copies, waits for them, and re-layouts  1.47 us

profile of v5, /device:TPU:0, one launch (start us, length us, event | category | flops | bytes accessed | tf_op | source)
XLA Modules:
  0.0 34.6 jit_solution(188974557354820778)
XLA Ops:
  0.0 33.1 %shard_map.109 = bf16[32,1024]{1,0:T(8,128)(2,1)} custom-call(bf16[32,2048]{1,0:T(8,128)(2,1)} %tok_hbm.1, s32[4,32]{1,0:T(4,128)} %bitcast.2, f32[4,32]{1,0:T(4,128)} %bitcast.3, bf16[2048]{0:T(1024)(128)(2,1)} %ngain_hbm.1, bf16[1,2048,1024]{2,1,0:T(8,128)(2,1)} %wg_hbm.1, bf16[1,2048,1024]{2,1,0:T(8,128)(2,1)} %wu_hbm.1, bf16[1,1024,2048]{2,1,0:T(8,128)(2,1)} %wd_hbm.1, ...), custom_call_target="tpu_custom_call" | custom-call | tf_op jit(solution)/shard_map/pallas_call | solution.py:350
  33.1 1.5 %copy.13 = bf16[32,1024]{1,0:T(8,128)(2,1)} copy(bf16[32,1024]{1,0:T(8,128)(2,1)} %shard_map.109) | data formatting | bytes 131072
